TPU v7x, 512 devices: a whole 4x4x16 slice. The times are simulated.
512 devices in a mesh: sp: 32 (over z, core), tp: 16 (over y, x).
Axes of the slice: x: 4, y: 4, z: 16, core: 2. Of those that a mesh axis runs over, the one named last changes fastest.
Arguments:
- queries: bfloat16 [8192, 1024], P('sp', 'tp'), may hold values from -250 to 250
- keys_values: bfloat16 [2, 8192, 256], P(None, 'sp'), may hold values from -8 to 8
- sink_logits: float32 [16], P('tp'), may hold values from 1 to 5
- proj_weight: bfloat16 [1024, 2048], P('tp'), may hold values from -0.75 to 0.75
- residual: bfloat16 [8192, 2048], P('sp', 'tp'), may hold values from -6 to 6
- norm_gain: float32 [2048], replicated, may hold values from 0.1 to 1.9
- routes: int32 [8192, 2], P('sp'), may hold values from 0 to 31, all different within a row; in each aligned block of 256 rows (0 to 255, 256 to 511, ...) at most 32 rows name the same one
- route_weights: float32 [8192, 2], P('sp'), may hold values from 0.2 to 1
- gate_weight: bfloat16 [32, 2048, 2048], P('sp', None, 'tp'), may hold values from -0.125 to 0.125
- up_weight: bfloat16 [32, 2048, 2048], P('sp', None, 'tp'), may hold values from -0.125 to 0.125
- down_weight: bfloat16 [32, 2048, 2048], P('sp', None, 'tp'), may hold values from -0.125 to 0.125
- shared_gate: bfloat16 [2048, 2048], P(None, 'tp'), may hold values from -0.125 to 0.125
- shared_up: bfloat16 [2048, 2048], P(None, 'tp'), may hold values from -0.125 to 0.125
- shared_down: bfloat16 [2048, 2048], P(None, 'tp'), may hold values from -0.125 to 0.125
Outputs:
- output: bfloat16 [8192, 2048], P('sp', 'tp')
Inputs may be any that keep to these rules, and one draw needn't show every extreme that they name: `routes`: the 2 experts of a position differ. In each aligned block of 256 positions no expert is named by more than 32 positions, and in some block one expert is named by exactly 32.
All inputs are finite; a program needn't handle non-finite values.
Results may differ from a plain program's by a relative error of at most 0.0067.
Values may be sent and summed in bfloat16 or wider, within the bound.
No kernel may reach another device: no remote copies, remote signals or barrier semaphores. Data moves between devices by JAX's collectives and lax.ppermute only.
A program may use at most 64 MiB of HBM per device.

v0:
```python
import jax
import jax.numpy as jnp
import numpy as np
from jax import lax
from jax.experimental import pallas as pl
from jax.experimental.pallas import tpu as pltpu
from jax.sharding import PartitionSpec as P


D = 2048
HEADS = 16
KV_HEADS = 4
HEAD_WIDTH = 64
WINDOW = 128
TOK_DEV = 256
N_SP = 32
N_TP = 16
CAP = 32
G = 4
ROWS = N_SP * CAP // G
OWN = TOK_DEV // G
ALL_ROWS = ROWS + OWN
TILE = D // N_TP
EPS = 1e-06
BF = jnp.bfloat16
F32 = jnp.float32


BOTH = ("sp", "tp")


def make_groups(along_r):
    groups = []
    for sp in range(N_SP):
        tiles = np.arange(N_TP).reshape(G, G)
        if (sp % 2 == 0) == along_r:
            tiles = tiles.T
        groups += [[sp * N_TP + int(t) for t in row] for row in tiles]
    return groups


R_GROUPS = make_groups(True)
H_GROUPS = make_groups(False)


def shifted(x, groups, step):
    pairs = [(g[i], g[(i + step) % G]) for g in groups for i in range(G)]
    return lax.ppermute(x, BOTH, pairs)


def swapped(x, groups):
    return lax.all_to_all(x, BOTH, 0, 0, tiled=True, axis_index_groups=groups)


def dot(a, b, dims=(((1,), (0,)), ((), ()))):
    return lax.dot_general(a, b, dims, preferred_element_type=F32)


VM = pl.BlockSpec(memory_space=pltpu.VMEM)
SM = pl.BlockSpec(memory_space=pltpu.SMEM)
PARAMS = pltpu.CompilerParams(vmem_limit_bytes=16 * 1024 * 1024)


def call(kernel, shapes, specs, scratch=()):
    return pl.pallas_call(
        kernel,
        out_shape=shapes,
        in_specs=specs,
        out_specs=jax.tree.map(lambda _: VM, shapes),
        scratch_shapes=list(scratch),
        compiler_params=PARAMS,
    )


def payload_kernel(sink, queries, proj, out):
    W = WINDOW
    pair = jnp.concatenate([queries[:W], queries[W:]], axis=1)
    logit = jnp.full((16, TILE), sink[0], F32)
    first = logit.astype(BF)
    rest = logit - first.astype(F32)
    second = rest.astype(BF)
    third = (rest - second.astype(F32)).astype(BF)
    lane = lax.broadcasted_iota(jnp.int32, (16, TILE), 1)
    parts = jnp.where(
        lane == 0, first.astype(F32), jnp.where(lane == 1, second.astype(F32), third.astype(F32))
    ).astype(BF)
    for t in range(N_TP):
        out[t, :W] = pair
        out[t, W : W + HEAD_WIDTH] = proj[:, t * TILE : (t + 1) * TILE]
        out[t, W + HEAD_WIDTH :] = parts


def route_kernel(routes_t, slots_out, pick_out):
    n = TOK_DEV
    experts = lax.broadcasted_iota(jnp.int32, (N_SP, n), 0)
    hit0 = (experts == routes_t[0:1, :]).astype(F32)
    hit1 = (experts == routes_t[1:2, :]).astype(F32)
    upper = (
        lax.broadcasted_iota(jnp.int32, (n, n), 0) < lax.broadcasted_iota(jnp.int32, (n, n), 1)
    ).astype(F32)
    earlier = dot((hit0 + hit1).astype(BF), upper.astype(BF))
    slot0 = routes_t[0:1, :] * CAP + jnp.sum(earlier * hit0, axis=0, keepdims=True).astype(jnp.int32)
    slot1 = routes_t[1:2, :] * CAP + jnp.sum(earlier * hit1, axis=0, keepdims=True).astype(jnp.int32)
    slots_out[0:1, :] = slot0
    slots_out[1:2, :] = slot1
    step = 256
    for j in range(0, N_SP * CAP, step):
        place = lax.broadcasted_iota(jnp.int32, (step, n), 0) + j
        pick = (place == slot0) | (place == slot1)
        pick_out[j : j + step, :] = pick.astype(F32).astype(BF)


def front_kernel(meta, recv, halo, kv, residual, pick, stream_out, picked_out, att):
    W, HW = WINDOW, HEAD_WIDTH
    row = lax.broadcasted_iota(jnp.int32, (G * W, W), 0) % W
    col = lax.broadcasted_iota(jnp.int32, (G * W, W), 1)
    before = col > row
    first = meta[4] == 0
    for b in range(2):
        for g in range(KV_HEADS):
            lanes = slice(g * HW, (g + 1) * HW)
            if b == 0:
                k_old, v_old = halo[0, :, lanes], halo[1, :, lanes]
            else:
                k_old, v_old = kv[0, :W, lanes], kv[1, :W, lanes]
            k_new, v_new = kv[0, b * W : (b + 1) * W, lanes], kv[1, b * W : (b + 1) * W, lanes]
            heads = [g * (HEADS // KV_HEADS) + i for i in range(HEADS // KV_HEADS)]
            q = jnp.concatenate([recv[h, :W, b * HW : (b + 1) * HW] for h in heads], axis=0)
            sink_rows = [recv[h, 192:193, :].astype(F32) for h in heads]
            sink = jnp.concatenate(
                [
                    jnp.broadcast_to(s[:, 0:1] + s[:, 1:2] + s[:, 2:3], (W, 1))
                    for s in sink_rows
                ],
                axis=0,
            )
            t_dims = (((1,), (1,)), ((), ()))
            s_old = dot(q, k_old, t_dims)
            if b == 0:
                s_old = jnp.where(first, -jnp.inf, s_old)
            score = jnp.where(before, s_old, dot(q, k_new, t_dims)) * HW ** (-0.5)
            top = jnp.maximum(jnp.max(score, axis=1, keepdims=True), sink)
            e = jnp.exp(score - top)
            den = jnp.sum(e, axis=1, keepdims=True) + jnp.exp(sink - top)
            p = e * (1.0 / den)
            p_old = jnp.where(before, p, 0.0).astype(BF)
            p_new = jnp.where(before, 0.0, p).astype(BF)
            a = (dot(p_old, v_old) + dot(p_new, v_new)).astype(BF)
            for i in range(0, len(heads), 2):
                pair = jnp.concatenate([a[i * W : (i + 1) * W], a[(i + 1) * W : (i + 2) * W]], axis=1)
                att[b * W : (b + 1) * W, heads[i] * HW : (heads[i] + 2) * HW] = pair
    weight = recv[:, 128:192, :].reshape(HEADS * HW, TILE)
    stream = (dot(att[...], weight) + residual[...].astype(F32)).astype(BF)
    stream_out[...] = stream
    picked_out[...] = dot(pick[...], stream).astype(BF)


def lanes_at(index):
    return pl.ds(pl.multiple_of(index * TILE, TILE), TILE)


def row_scale(x):
    return lax.rsqrt(jnp.sum(x * x, axis=1, keepdims=True) / D + EPS)


def gated(scale, both):
    g = scale * both[:, :TILE]
    u = scale * both[:, TILE:]
    return (g / (1.0 + jnp.exp(-g)) * u).astype(BF)


def spread_kernel(meta, arrived, stream, out):
    for t in range(N_TP):
        r = jnp.where(meta[2] == G, t // G, t % G)
        out[t, :ROWS] = arrived[r]
        out[t, ROWS:] = stream[r]


HALF = D // 2


def both_halves(x, top, bottom):
    return dot(x[:, :HALF], top) + dot(x[:, HALF:], bottom)


def hidden_kernel(rows, own, back, top, bottom, ahead, out, x):
    for t in range(N_TP):
        x[:, t * TILE : (t + 1) * TILE] = rows[t]
    for at, part in ((0, slice(0, ROWS)), (3 * TILE, slice(ROWS, ALL_ROWS))):
        full = x[part, :]
        lanes = slice(at, at + 2 * TILE)
        scale = row_scale(full.astype(F32))
        for s in range(G):
            if s == 2:
                sums = both_halves(full, top[:, lanes], bottom[:, lanes])
            else:
                sums = dot(full, (own, back, None, ahead)[s][:, lanes])
            result = gated(scale, sums)
            for k in range(G):
                out[k, part, s * TILE : (s + 1) * TILE] = result


def down_kernel(meta, hidden, own, back, top, bottom, ahead, out, x, w):
    places = [lax.rem(meta[0] + (G - s), G) for s in range(G)]
    for s in range(G):
        for h in range(G):
            tile = places[s] * meta[2] + h * meta[3]
            x[:, lanes_at(tile)] = hidden[h, :, s * TILE : (s + 1) * TILE]
    for at, part in ((2 * TILE, slice(0, ROWS)), (5 * TILE, slice(ROWS, ALL_ROWS))):
        lanes = slice(at, at + TILE)
        for s in range(G):
            cols = slice(s * TILE, (s + 1) * TILE)
            if s == 2:
                w[:HALF, cols] = top[:, lanes]
                w[HALF:, cols] = bottom[:, lanes]
            else:
                w[:, cols] = (own, back, None, ahead)[s][:, lanes]
        result = dot(x[part, :], w[...]).astype(BF)
        for s in range(G):
            out[places[s], part] = result[:, s * TILE : (s + 1) * TILE]


def return_kernel(parts, out):
    for r in range(G):
        out[r] = parts[r, :ROWS]


def combine_kernel(back, slots, weights_t, stream, parts, out):
    n = TOK_DEV
    own = jnp.concatenate([parts[r, ROWS:] for r in range(G)], axis=0)
    total = stream[...].astype(F32) + own.astype(F32)
    step = 256
    dims = (((0,), (0,)), ((), ()))
    for j in range(0, N_SP * CAP, step):
        place = lax.broadcasted_iota(jnp.int32, (step, n), 0) + j
        mix = jnp.where(place == slots[0:1, :], weights_t[0:1, :], 0.0) + jnp.where(
            place == slots[1:2, :], weights_t[1:2, :], 0.0
        )
        high = mix.astype(BF)
        low = (mix - high.astype(F32)).astype(BF)
        piece = back[j : j + step, :]
        total = total + dot(high, piece, dims) + dot(low, piece, dims)
    out[...] = total.astype(BF)


def layer(
    queries,
    keys_values,
    sink_logits,
    proj_weight,
    residual,
    norm_gain,
    routes,
    route_weights,
    gate_weight,
    up_weight,
    down_weight,
    shared_gate,
    shared_up,
    shared_down,
):
    sds = jax.ShapeDtypeStruct
    sp = lax.axis_index("sp")
    tp = lax.axis_index("tp")
    odd = lax.rem(sp, 2)
    high, low = tp // G, lax.rem(tp, G)
    r = jnp.where(odd == 0, high, low)
    h = jnp.where(odd == 0, low, high)
    meta = jnp.stack([r, h, jnp.where(odd == 0, G, 1), jnp.where(odd == 0, 1, G), sp]).astype(
        jnp.int32
    )

    payload = call(
        payload_kernel, sds((N_TP, WINDOW + HEAD_WIDTH + 16, TILE), BF), [SM, VM, VM]
    )(sink_logits, queries, proj_weight)
    recv = lax.all_to_all(payload, "tp", 0, 0, tiled=True)
    halo = lax.ppermute(
        keys_values[:, TOK_DEV - WINDOW :, :], "sp", [(i, i + 1) for i in range(N_SP - 1)]
    )

    gain = norm_gain[:, None]

    def packed(gate, up, down):
        gate_eff = (gain * gate.astype(F32)).astype(BF)
        up_eff = (gain * up.astype(F32)).astype(BF)
        return [gate_eff, up_eff, down]

    own = jnp.concatenate(
        packed(gate_weight[0], up_weight[0], down_weight[0])
        + packed(shared_gate, shared_up, shared_down),
        axis=1,
    )
    behind = shifted(own, R_GROUPS, 1)
    ahead = shifted(own, R_GROUPS, 3)
    top = shifted(behind[:HALF], R_GROUPS, 1)
    bottom = shifted(ahead[HALF:], R_GROUPS, 3)
    weights = (own, behind, top, bottom, ahead)

    slots, pick = call(
        route_kernel,
        (sds((2, TOK_DEV), jnp.int32), sds((N_SP * CAP, TOK_DEV), BF)),
        [VM],
    )(routes.T)
    stream, picked = call(
        front_kernel,
        (sds((TOK_DEV, TILE), BF), sds((N_SP * CAP, TILE), BF)),
        [SM, VM, VM, VM, VM, VM],
        [pltpu.VMEM((TOK_DEV, HEADS * HEAD_WIDTH), BF)],
    )(meta, recv, halo, keys_values, residual, pick)

    arrived = lax.all_to_all(picked.reshape(N_SP, CAP, TILE), "sp", 0, 0, tiled=True)

    sent = call(spread_kernel, sds((N_TP, ALL_ROWS, TILE), BF), [SM, VM, VM])(
        meta, arrived.reshape(G, ROWS, TILE), stream.reshape(G, OWN, TILE)
    )
    rows = lax.all_to_all(sent, "tp", 0, 0, tiled=True)

    hidden = call(
        hidden_kernel,
        sds((G, ALL_ROWS, G * TILE), BF),
        [VM] * 6,
        [pltpu.VMEM((ALL_ROWS, D), BF)],
    )(rows, *weights)
    hidden = swapped(hidden, H_GROUPS)

    parts = call(
        down_kernel,
        sds((G, ALL_ROWS, TILE), BF),
        [SM] + [VM] * 6,
        [pltpu.VMEM((ALL_ROWS, D), BF), pltpu.VMEM((D, G * TILE), BF)],
    )(meta, hidden, *weights)
    parts = swapped(parts, R_GROUPS)

    outgoing = call(return_kernel, sds((G, ROWS, TILE), BF), [VM])(parts)
    back = lax.all_to_all(outgoing.reshape(N_SP, CAP, TILE), "sp", 0, 0, tiled=True)
    return call(combine_kernel, sds((TOK_DEV, TILE), BF), [VM, VM, VM, VM, VM])(
        back.reshape(N_SP * CAP, TILE), slots, route_weights.T, stream, parts
    )


def solution(mesh):
    placed = (
        P("sp", "tp"),
        P(None, "sp", None),
        P("tp"),
        P("tp", None),
        P("sp", "tp"),
        P(),
        P("sp", None),
        P("sp", None),
        P("sp", None, "tp"),
        P("sp", None, "tp"),
        P("sp", None, "tp"),
        P(None, "tp"),
        P(None, "tp"),
        P(None, "tp"),
    )
    return jax.shard_map(
        layer, mesh=mesh, in_specs=placed, out_specs=P("sp", "tp"), check_vma=False
    )
```

profile of v0, /device:TPU:1, one launch (start us, length us, event | category | flops | bytes accessed | tf_op | source)
XLA Modules:
  0.0 210.6 jit_solution(1713076418455702428)
XLA Ops:
  0.0 0.0 copy-start.13
  0.0 0.0 copy-start.15
  0.0 2.4 %fusion.4 = bf16[2048,768]{1,0:T(8,128)(2,1)} fusion(bf16[1,2048,128]{2,1,0:T(8,128)(2,1)} %param.22, f32[2048]{0:T(1024)} %param.19), kind=kLoop, calls=%fused_computation.8 | loop fusion | flops 786431 | bytes 1056768
  2.4 2.2 %fusion.5 = bf16[2048,768]{1,0:T(8,128)(2,1)} fusion(bf16[2048,768]{1,0:T(8,128)(2,1)} %fusion.4, bf16[1,2048,128]{2,1,0:T(8,128)(2,1)} %param.23, f32[2048]{0:T(1024)} %param.19), kind=kLoop, calls=%fused_computation.9 | loop fusion | flops 786432 | bytes 1056768
  4.6 1.9 bitcast_dynamic-update-slice_fusion
  6.6 1.2 fusion.2
  7.8 1.2 fusion.3
  8.9 0.9 constant_dynamic-update-slice_fusion.own
  9.8 5.2 %collective-permute-start.3 = (bf16[2048,768]{1,0:T(8,128)(2,1)}, bf16[2048,768]{1,0:T(8,128)(2,1)S(1)}, u32[]{:S(2)}, u32[]{:S(2)}) collective-permute-start(bf16[2048,768]{1,0:T(8,128)(2,1)} %constant_dynamic-update-slice_fusion.own), channel_id=1, source_target_pairs={{0,12},{4,0},{8,4},{12,8},{1,13},{5,1},{9,5},{13,9},{2,14},{6,2},{... | collective-permute-start | bytes 9437192 | tf_op jit(solution)/shard_map/ppermute | solution.py:48
  15.0 1.9 collective-permute-start.1
  17.6 0.0 copy-done.15
  17.6 0.1 copy.15.queries
  17.7 0.0 copy-start.5
  17.7 0.9 copy-done.5
  18.7 0.1 shard_map.136
  18.8 0.9 copy-done
  19.7 6.7 %all-to-all-start = ((bf16[16,208,128]{2,1,0:T(8,128)(2,1)}), bf16[16,208,128]{2,1,0:T(8,128)(2,1)}, u32[]{:S(2)}, u32[]{:S(2)}) async-start(bf16[16,208,128]{2,1,0:T(8,128)(2,1)} %copy-done), calls=%async_computation | async-start | bytes 1703936 | tf_op jit(solution)/shard_map/all_to_all | solution.py:276
  26.5 0.7 slice.9
  27.1 5.0 %collective-permute-start = (bf16[2,128,256]{2,1,0:T(8,128)(2,1)}, bf16[2,128,256]{2,1,0:T(8,128)(2,1)S(1)}, u32[]{:S(2)}, u32[]{:S(2)}) collective-permute-start(bf16[2,128,256]{2,1,0:T(8,128)(2,1)} %slice.9), channel_id=1, source_target_pairs={{0,16},{16,32},{32,48},{48,64},{64,80},{80,96},{96,112},{112,128},... | collective-permute-start | bytes 393224 | tf_op jit(solution)/shard_map/ppermute | solution.py:277
  32.2 0.3 shard_map.137
  32.6 0.8 copy-done.2
  33.4 0.1 stack.23.meta
  33.5 0.9 collective-permute-done.halo
  34.4 0.6 copy-done.6
  35.1 30.4 %all-to-all-done.recv = bf16[16,208,128]{2,1,0:T(8,128)(2,1)} async-done(((bf16[16,208,128]{2,1,0:T(8,128)(2,1)}), bf16[16,208,128]{2,1,0:T(8,128)(2,1)}, u32[]{:S(2)}, u32[]{:S(2)}) %all-to-all-start) | async-done | bytes 852000 | tf_op jit(solution)/shard_map/all_to_all | solution.py:276
  65.5 1.0 copy-done.3
  66.5 0.9 copy-done.7
  67.4 0.8 copy-done.8
  68.2 8.4 %shard_map.138 = (bf16[256,128]{1,0:T(8,128)(2,1)S(1)}, bf16[1024,128]{1,0:T(8,128)(2,1)S(1)}) custom-call(s32[5]{0:T(128)S(1)} %stack.23.meta, bf16[16,208,128]{2,1,0:T(8,128)(2,1)} %all-to-all-done.recv, bf16[2,128,256]{2,1,0:T(8,128)(2,1)S(1)} %copy-done.7, bf16[2,256,256]{2,1,0:T(8,128)(2,1)S(1)} %copy-done.1, bf16[256,128]{1,0:T(8,128)(2,1)S(1)} %copy-done.8, ...), custom_call_target="tpu_custom_call" | custom-call | tf_op jit(solution)/shard_map/pallas_call | solution.py:304
  76.7 0.7 copy-done.4
  77.4 15.4 %all-to-all-start.1 = ((bf16[32,32,128]{2,1,0:T(8,128)(2,1)}), bf16[32,32,128]{2,1,0:T(8,128)(2,1)S(1)}, u32[]{:S(2)}, u32[]{:S(2)}) async-start(bf16[32,32,128]{2,1,0:T(8,128)(2,1)} %bitcast.23), calls=%async_computation.1 | async-start | bytes 524288 | tf_op jit(solution)/shard_map/all_to_all | solution.py:311
  92.7 0.0 collective-permute-done.3.ahead
  92.8 1.3 slice.13
  94.0 4.8 %collective-permute-start.4 = (bf16[1024,768]{1,0:T(8,128)(2,1)}, bf16[1024,768]{1,0:T(8,128)(2,1)}, u32[]{:S(2)}, u32[]{:S(2)}) collective-permute-start(bf16[1024,768]{1,0:T(8,128)(2,1)} %slice.13), channel_id=1, source_target_pairs={{0,12},{4,0},{8,4},{12,8},{1,13},{5,1},{9,5},{13,9},{2,14},{6,2},{... | collective-permute-start | bytes 4718600 | tf_op jit(solution)/shard_map/ppermute | solution.py:48
  98.9 0.0 collective-permute-done.1.back
  98.9 2.7 %slice.12 = bf16[1024,768]{1,0:T(8,128)(2,1)} slice(bf16[2048,768]{1,0:T(8,128)(2,1)} %collective-permute-done.1.back), slice={[0:1024], [0:768]} | slice | bytes 3145728 | tf_op jit(solution)/shard_map/slice | solution.py:295
  101.6 1.9 collective-permute-start.2
  103.5 11.5 %all-to-all-done.1 = bf16[32,32,128]{2,1,0:T(8,128)(2,1)S(1)} async-done(((bf16[32,32,128]{2,1,0:T(8,128)(2,1)}), bf16[32,32,128]{2,1,0:T(8,128)(2,1)S(1)}, u32[]{:S(2)}, u32[]{:S(2)}) %all-to-all-start.1) | async-done | bytes 262176 | tf_op jit(solution)/shard_map/all_to_all | solution.py:311
  115.0 0.6 shard_map.139
  115.6 23.6 %all_to_all.30.rows = bf16[16,320,128]{2,1,0:T(8,128)(2,1)S(1)} all-to-all(bf16[16,320,128]{2,1,0:T(8,128)(2,1)S(1)} %shard_map.139), channel_id=1, replica_groups=mesh['sp'=32,'tp'=16] {'tp'}, dimensions={0} | all-to-all | bytes 2621440 | tf_op jit(solution)/shard_map/all_to_all | solution.py:316
  139.2 0.0 collective-permute-done.4.bottom
  139.2 0.0 collective-permute-done.2.top
  139.2 5.8 %shard_map.140 = bf16[4,320,512]{2,1,0:T(8,128)(2,1)S(1)} custom-call(bf16[16,320,128]{2,1,0:T(8,128)(2,1)S(1)} %all_to_all.30.rows, bf16[2048,768]{1,0:T(8,128)(2,1)} %constant_dynamic-update-slice_fusion.own, bf16[2048,768]{1,0:T(8,128)(2,1)} %collective-permute-done.1.back, bf16[1024,768]{1,0:T(8,128)(2,1)} %collective-permute-done.2.top, ...), custom_call_target="tpu_custom_call" | custom-call | tf_op jit(solution)/shard_map/pallas_call | solution.py:318
  145.0 13.9 %all_to_all.31.hidden = bf16[4,320,512]{2,1,0:T(8,128)(2,1)S(1)} all-to-all(bf16[4,320,512]{2,1,0:T(8,128)(2,1)S(1)} %shard_map.140), channel_id=1, replica_groups={{0,1,2,3},{4,5,6,7},{8,9,10,11},{12,13,14,15},{16,20,24,28},{17,21,25,2..., dimensions={0} | all-to-all | bytes 2621440 | tf_op jit(solution)/shard_map/all_to_all | solution.py:52
  158.9 5.6 %shard_map.141 = bf16[4,320,128]{2,1,0:T(8,128)(2,1)S(1)} custom-call(s32[5]{0:T(128)S(1)} %stack.23.meta, bf16[4,320,512]{2,1,0:T(8,128)(2,1)S(1)} %all_to_all.31.hidden, bf16[2048,768]{1,0:T(8,128)(2,1)} %constant_dynamic-update-slice_fusion.own, bf16[2048,768]{1,0:T(8,128)(2,1)} %collective-permute-done.1.back, ...), custom_call_target="tpu_custom_call" | custom-call | tf_op jit(solution)/shard_map/pallas_call | solution.py:326
  164.6 8.3 %all_to_all.32.parts = bf16[4,320,128]{2,1,0:T(8,128)(2,1)S(1)} all-to-all(bf16[4,320,128]{2,1,0:T(8,128)(2,1)S(1)} %shard_map.141), channel_id=1, replica_groups={{0,4,8,12},{1,5,9,13},{2,6,10,14},{3,7,11,15},{16,17,18,19},{20,21,22,2..., dimensions={0} | all-to-all | bytes 655360 | tf_op jit(solution)/shard_map/all_to_all | solution.py:52
  172.8 36.6 %all_to_all.33 = bf16[32,32,128]{2,1,0:T(8,128)(2,1)S(1)} all-to-all(bf16[32,32,128]{2,1,0:T(8,128)(2,1)S(1)} %bitcast.20), channel_id=1, replica_groups=mesh['sp'=32,'tp'=16] {'sp'}, dimensions={0} | all-to-all | bytes 524288 | tf_op jit(solution)/shard_map/all_to_all | solution.py:335
  209.4 1.2 shard_map.143
  (21 shorter events, 0.1 us)
Async XLA Ops:
  0.0 6.6 %copy-start.14 = (f32[2048]{0:T(1024)S(1)}, f32[2048]{0:T(1024)}, u32[]{:S(2)}) copy-start(f32[2048]{0:T(1024)} %param.19) | copy-start | bytes 24580
  0.0 6.6 %copy-start.11 = (bf16[2048,128]{1,0:T(8,128)(2,1)S(1)}, bf16[2048,128]{1,0:T(8,128)(2,1)}, u32[]{:S(2)}) copy-start(bf16[2048,128]{1,0:T(8,128)(2,1)} %param.25) | copy-start | bytes 1572868
  0.0 7.8 %copy-start.12 = (bf16[2048,128]{1,0:T(8,128)(2,1)S(1)}, bf16[2048,128]{1,0:T(8,128)(2,1)}, u32[]{:S(2)}) copy-start(bf16[2048,128]{1,0:T(8,128)(2,1)} %param.26) | copy-start | bytes 1572868
  0.0 8.9 %copy-start.13 = (bf16[2048,128]{1,0:T(8,128)(2,1)S(1)}, bf16[2048,128]{1,0:T(8,128)(2,1)}, u32[]{:S(2)}) copy-start(bf16[2048,128]{1,0:T(8,128)(2,1)} %param.27) | copy-start | bytes 1572868
  0.0 17.6 %copy-start.15 = (bf16[256,64]{0,1:T(8,128)(2,1)S(1)}, bf16[256,64]{0,1:T(8,128)(2,1)}, u32[]{:S(2)}) copy-start(bf16[256,64]{0,1:T(8,128)(2,1)} %param.14) | copy-start | bytes 98308
  6.6 19.9 %copy-start.1 = (bf16[2,256,256]{2,1,0:T(8,128)(2,1)S(1)}, bf16[2,256,256]{2,1,0:T(8,128)(2,1)}, u32[]{:S(2)}) copy-start(bf16[2,256,256]{2,1,0:T(8,128)(2,1)} %kv.1) | copy-start | bytes 786436
  6.6 25.6 %copy-start.10 = (s32[256,2]{0,1:T(2,128)S(1)}, s32[256,2]{0,1:T(2,128)}, u32[]{:S(2)}) copy-start(s32[256,2]{0,1:T(2,128)} %param.20) | copy-start | bytes 6148
  9.8 82.9 %collective-permute-start.3 = (bf16[2048,768]{1,0:T(8,128)(2,1)}, bf16[2048,768]{1,0:T(8,128)(2,1)S(1)}, u32[]{:S(2)}, u32[]{:S(2)}) collective-permute-start(bf16[2048,768]{1,0:T(8,128)(2,1)} %constant_dynamic-update-slice_fusion.own), channel_id=1, source_target_pairs={{0,12},{4,0},{8,4},{12,8},{1,13},{5,1},{9,5},{13,9},{2,14},{6,2},{... | collective-permute-start | bytes 9437192 | tf_op jit(solution)/shard_map/ppermute | solution.py:48
  15.0 83.9 %collective-permute-start.1 = (bf16[2048,768]{1,0:T(8,128)(2,1)}, bf16[2048,768]{1,0:T(8,128)(2,1)}, u32[]{:S(2)}, u32[]{:S(2)}) collective-permute-start(bf16[2048,768]{1,0:T(8,128)(2,1)} %constant_dynamic-update-slice_fusion.own), channel_id=1, source_target_pairs={{0,4},{4,8},{8,12},{12,0},{1,5},{5,9},{9,13},{13,1},{2,6},{6,10},{... | collective-permute-start | bytes 9437192 | tf_op jit(solution)/shard_map/ppermute | solution.py:48
  17.7 1.0 copy-start.5
  18.8 0.9 copy-start
  19.7 45.7 %all-to-all-start = ((bf16[16,208,128]{2,1,0:T(8,128)(2,1)}), bf16[16,208,128]{2,1,0:T(8,128)(2,1)}, u32[]{:S(2)}, u32[]{:S(2)}) async-start(bf16[16,208,128]{2,1,0:T(8,128)(2,1)} %copy-done), calls=%async_computation | async-start | bytes 1703936 | tf_op jit(solution)/shard_map/all_to_all | solution.py:276
  27.1 7.3 %collective-permute-start = (bf16[2,128,256]{2,1,0:T(8,128)(2,1)}, bf16[2,128,256]{2,1,0:T(8,128)(2,1)S(1)}, u32[]{:S(2)}, u32[]{:S(2)}) collective-permute-start(bf16[2,128,256]{2,1,0:T(8,128)(2,1)} %slice.9), channel_id=1, source_target_pairs={{0,16},{16,32},{32,48},{48,64},{64,80},{80,96},{96,112},{112,128},... | collective-permute-start | bytes 393224 | tf_op jit(solution)/shard_map/ppermute | solution.py:277
  32.5 0.8 copy-start.2
  34.4 0.6 copy-start.6
  65.5 1.0 copy-start.3
  66.5 0.9 copy-start.7
  67.4 0.8 copy-start.8
  76.7 0.7 copy-start.4
  77.4 37.6 %all-to-all-start.1 = ((bf16[32,32,128]{2,1,0:T(8,128)(2,1)}), bf16[32,32,128]{2,1,0:T(8,128)(2,1)S(1)}, u32[]{:S(2)}, u32[]{:S(2)}) async-start(bf16[32,32,128]{2,1,0:T(8,128)(2,1)} %bitcast.23), calls=%async_computation.1 | async-start | bytes 524288 | tf_op jit(solution)/shard_map/all_to_all | solution.py:311
  94.0 45.2 %collective-permute-start.4 = (bf16[1024,768]{1,0:T(8,128)(2,1)}, bf16[1024,768]{1,0:T(8,128)(2,1)}, u32[]{:S(2)}, u32[]{:S(2)}) collective-permute-start(bf16[1024,768]{1,0:T(8,128)(2,1)} %slice.13), channel_id=1, source_target_pairs={{0,12},{4,0},{8,4},{12,8},{1,13},{5,1},{9,5},{13,9},{2,14},{6,2},{... | collective-permute-start | bytes 4718600 | tf_op jit(solution)/shard_map/ppermute | solution.py:48
  101.6 37.7 %collective-permute-start.2 = (bf16[1024,768]{1,0:T(8,128)(2,1)}, bf16[1024,768]{1,0:T(8,128)(2,1)}, u32[]{:S(2)}, u32[]{:S(2)}) collective-permute-start(bf16[1024,768]{1,0:T(8,128)(2,1)} %slice.12), channel_id=1, source_target_pairs={{0,4},{4,8},{8,12},{12,0},{1,5},{5,9},{9,13},{13,1},{2,6},{6,10},{... | collective-permute-start | bytes 4718600 | tf_op jit(solution)/shard_map/ppermute | solution.py:48
  158.9 50.5 %copy-start.9 = (f32[256,2]{0,1:T(2,128)S(1)}, f32[256,2]{0,1:T(2,128)}, u32[]{:S(2)}) copy-start(f32[256,2]{0,1:T(2,128)} %param.21) | copy-start | bytes 6148
where the time goes:
time: 211 us
  blocking collectives  82.3 us (39%)
  waiting for transfers between devices  42.9 us (20%)
  starting transfers between devices  41 us (19%)
  Pallas kernels  22.2 us (11%)
  local copies, waits for them, and re-layouts  14.5 us (7%)
  other arithmetic  6.95 us (3%)
    all_to_all x1, blocking collectives, layer(): lax.all_to_all(outgoing.reshape(N_SP, CAP, TILE), 'sp', 0, 0, tiled=True)  36.6 us
    all_to_all x1, waiting for transfers between devices, layer(): recv = lax.all_to_all(payload, 'tp', 0, 0, tiled=True)  30.4 us
    all_to_all x1, blocking collectives, layer(): rows = lax.all_to_all(sent, 'tp', 0, 0, tiled=True)  23.6 us
    all_to_all x2, blocking collectives, swapped(): return lax.all_to_all(x, BOTH, 0, 0, tiled=True, axis_index_groups=groups)  22.1 us
    all_to_all x1, starting transfers between devices, layer(): lax.all_to_all(picked.reshape(N_SP, CAP, TILE), 'sp', 0, 0, tiled=True)  15.4 us
    ppermute x4, starting transfers between devices, shifted(): return lax.ppermute(x, BOTH, pairs)  13.9 us
    all_to_all x1, waiting for transfers between devices, layer(): lax.all_to_all(picked.reshape(N_SP, CAP, TILE), 'sp', 0, 0, tiled=True)  11.5 us
    unnamed x34, local copies, waits for them, and re-layouts  8.92 us
  transfers between devices with their start and end apart: 7, of which 3 were waited for; matrix products, arithmetic and copies ran while one was open for 2% of the time, Pallas kernels for 5%

commit v1 on v0

v1 whole, which is shorter than its diff:
```python
import jax
import jax.numpy as jnp
import numpy as np
from jax import lax
from jax.experimental import pallas as pl
from jax.experimental.pallas import tpu as pltpu
from jax.sharding import PartitionSpec as P


D = 2048
HEADS = 16
KV_HEADS = 4
HEAD_WIDTH = 64
WINDOW = 128
TOK_DEV = 256
N_SP = 32
N_TP = 16
CAP = 32
G = 4
ROWS = N_SP * CAP // G
OWN = TOK_DEV // G
ALL_ROWS = ROWS + OWN
TILE = D // N_TP
EPS = 1e-06
HALF = D // 2
BF = jnp.bfloat16
F32 = jnp.float32


BOTH = ("sp", "tp")


def make_groups(along_r):
    groups = []
    for sp in range(N_SP):
        tiles = np.arange(N_TP).reshape(G, G)
        if (sp % 2 == 0) == along_r:
            tiles = tiles.T
        groups += [[sp * N_TP + int(t) for t in row] for row in tiles]
    return groups


R_GROUPS = make_groups(True)
H_GROUPS = make_groups(False)


def shifted(x, groups, step):
    pairs = [(g[i], g[(i + step) % G]) for g in groups for i in range(G)]
    return lax.ppermute(x, BOTH, pairs)


def swapped(x, groups):
    return lax.all_to_all(x, BOTH, 0, 0, tiled=True, axis_index_groups=groups)


def dot(a, b, dims=(((1,), (0,)), ((), ()))):
    return lax.dot_general(a, b, dims, preferred_element_type=F32)


VM = pl.BlockSpec(memory_space=pltpu.VMEM)
SM = pl.BlockSpec(memory_space=pltpu.SMEM)
HB = pl.BlockSpec(memory_space=pltpu.HBM)
PARAMS = pltpu.CompilerParams(vmem_limit_bytes=24 * 1024 * 1024)


def call(kernel, shapes, specs, scratch=(), outs=None):
    return pl.pallas_call(
        kernel,
        out_shape=shapes,
        in_specs=specs,
        out_specs=outs or jax.tree.map(lambda _: VM, shapes),
        scratch_shapes=list(scratch),
        compiler_params=PARAMS,
    )


def payload_kernel(sink, queries_t, proj_at, out, proj, sem):
    W = WINDOW
    copy = pltpu.make_async_copy(proj_at, proj, sem)
    copy.start()
    pair = jnp.concatenate([queries_t[:, :W], queries_t[:, W:]], axis=0).T
    logit = jnp.full((16, TILE), sink[0], F32)
    first = logit.astype(BF)
    rest = logit - first.astype(F32)
    second = rest.astype(BF)
    third = (rest - second.astype(F32)).astype(BF)
    lane = lax.broadcasted_iota(jnp.int32, (16, TILE), 1)
    parts = jnp.where(
        lane == 0, first.astype(F32), jnp.where(lane == 1, second.astype(F32), third.astype(F32))
    ).astype(BF)
    copy.wait()
    for t in range(N_TP):
        out[t, :W] = pair
        out[t, W : W + HEAD_WIDTH] = proj[:, t * TILE : (t + 1) * TILE]
        out[t, W + HEAD_WIDTH :] = parts


def prep_kernel(
    gain, gate, up, down, s_gate, s_up, s_down, top, bottom, raw, scaled, sems
):
    def lanes(j):
        return slice(j * TILE, (j + 1) * TILE)

    halves = ((top, slice(0, HALF)), (bottom, slice(HALF, D)))

    scale_from = ((0, gate), (1, up), (3, s_gate), (4, s_up))
    loads = [pltpu.make_async_copy(ref, raw.at[i], sems.at[i]) for i, (_, ref) in enumerate(scale_from)]
    moves = [
        pltpu.make_async_copy(ref.at[rows], out.at[:, lanes(j)], sems.at[4 + 2 * i + k])
        for i, (j, ref) in enumerate(((2, down), (5, s_down)))
        for k, (out, rows) in enumerate(halves)
    ]
    for copy in loads + moves:
        copy.start()
    columns = [
        jnp.broadcast_to(gain[k : k + 1, :], (TILE, TILE)).T for k in range(D // TILE)
    ]
    stores = []
    for i, (j, _) in enumerate(scale_from):
        loads[i].wait()
        for k in range(D // TILE):
            rows = slice(k * TILE, (k + 1) * TILE)
            scaled[i, rows, :] = (columns[k] * raw[i, rows, :].astype(F32)).astype(BF)
        for k, (out, rows) in enumerate(halves):
            target = out.at[:, lanes(j)]
            stores.append(
                pltpu.make_async_copy(scaled.at[i, rows], target, sems.at[8 + 2 * i + k])
            )
            stores[-1].start()
    for copy in moves + stores:
        copy.wait()


def route_mask(routes_t, slots_out, pick):
    n = TOK_DEV
    experts = lax.broadcasted_iota(jnp.int32, (N_SP, n), 0)
    hit0 = (experts == routes_t[0:1, :]).astype(F32)
    hit1 = (experts == routes_t[1:2, :]).astype(F32)
    upper = (
        lax.broadcasted_iota(jnp.int32, (n, n), 0) < lax.broadcasted_iota(jnp.int32, (n, n), 1)
    ).astype(F32)
    earlier = dot((hit0 + hit1).astype(BF), upper.astype(BF))
    slot0 = routes_t[0:1, :] * CAP + jnp.sum(earlier * hit0, axis=0, keepdims=True).astype(jnp.int32)
    slot1 = routes_t[1:2, :] * CAP + jnp.sum(earlier * hit1, axis=0, keepdims=True).astype(jnp.int32)
    slots_out[0:1, :] = slot0
    slots_out[1:2, :] = slot1
    step = 256
    for j in range(0, N_SP * CAP, step):
        place = lax.broadcasted_iota(jnp.int32, (step, n), 0) + j
        hit = (place == slot0) | (place == slot1)
        pick[j : j + step, :] = hit.astype(F32).astype(BF)


def front_kernel(
    meta, routes_t, recv_at, halo_at, kv_at, residual_at, stream_out, picked_at, slots_out,
    recv, halo, kv, residual, pick, att, picked, sems,
):
    W, HW = WINDOW, HEAD_WIDTH
    pairs = ((kv_at, kv), (halo_at, halo), (recv_at, recv), (residual_at, residual))
    copies = [pltpu.make_async_copy(a, b, sems.at[i]) for i, (a, b) in enumerate(pairs)]
    for copy in copies:
        copy.start()
    route_mask(routes_t, slots_out, pick)
    for copy in copies[:3]:
        copy.wait()
    row = lax.broadcasted_iota(jnp.int32, (G * W, W), 0) % W
    col = lax.broadcasted_iota(jnp.int32, (G * W, W), 1)
    before = col > row
    left = lax.broadcasted_iota(jnp.int32, (W, W), 1) < HW
    first = meta[4] == 0
    nothing = jnp.zeros((W, HW), BF)
    t_dims = (((1,), (1,)), ((), ()))
    for g in range(KV_HEADS):
        lanes = slice(g * HW, (g + 1) * HW)
        blocks = [halo[:, :, lanes], kv[:, :W, lanes], kv[:, W:, lanes]]
        values = [jnp.concatenate([v[1], v[1]], axis=1) for v in blocks]
        q = recv[g * G : (g + 1) * G, :W, :].reshape(G * W, TILE) * BF(HW ** (-0.5))
        sink = jnp.concatenate(
            [
                jnp.broadcast_to(jnp.sum(recv[g * G + i, W + HW : W + HW + 1, :3].astype(F32), axis=1, keepdims=True), (W, 1))
                for i in range(G)
            ],
            axis=0,
        )
        for b in range(2):
            keys = [
                jnp.concatenate([k[0], nothing] if b == 0 else [nothing, k[0]], axis=1)
                for k in blocks[b : b + 2]
            ]
            s_old = dot(q, keys[0], t_dims)
            if b == 0:
                s_old = jnp.where(first, -jnp.inf, s_old)
            score = jnp.where(before, s_old, dot(q, keys[1], t_dims))
            top = jnp.maximum(jnp.max(score, axis=1, keepdims=True), sink)
            e = jnp.exp(score - top)
            den = jnp.sum(e, axis=1, keepdims=True) + jnp.exp(sink - top)
            p = e * (1.0 / den)
            p_old = jnp.where(before, p, 0.0).astype(BF)
            p_new = jnp.where(before, 0.0, p).astype(BF)
            a = (dot(p_old, values[b]) + dot(p_new, values[b + 1])).astype(F32)
            for i in range(0, G, 2):
                both = jnp.where(left, a[i * W : (i + 1) * W], a[(i + 1) * W : (i + 2) * W])
                h = g * G + i
                att[b * W : (b + 1) * W, h * HW : (h + 2) * HW] = both.astype(BF)
    copies[3].wait()
    weight = recv[:, W : W + HW, :].reshape(HEADS * HW, TILE)
    stream = (dot(att[...], weight) + residual[...].astype(F32)).astype(BF)
    stream_out[...] = stream
    sends = []
    step = 512
    for i in range(N_SP * CAP // step):
        rows = slice(i * step, (i + 1) * step)
        picked[rows, :] = dot(pick[rows, :], stream).astype(BF)
        sends.append(pltpu.make_async_copy(picked.at[rows], picked_at.at[rows], sems.at[4 + i]))
        sends[-1].start()
    for send in sends:
        send.wait()


def lanes_at(index):
    return pl.ds(pl.multiple_of(index * TILE, TILE), TILE)


def row_scale(x):
    return lax.rsqrt(jnp.sum(x * x, axis=1, keepdims=True) / D + EPS)


def gated(scale, both):
    g = scale * both[:, :TILE]
    u = scale * both[:, TILE:]
    return (g / (1.0 + jnp.exp(-g)) * u).astype(BF)


def spread_kernel(meta, arrived, stream, out):
    for t in range(N_TP):
        r = jnp.where(meta[2] == G, t // G, t % G)
        out[t, :ROWS] = arrived[r]
        out[t, ROWS:] = stream[r]


def piece_copies(refs, lanes, target, sems):
    high, low = slice(0, HALF), slice(HALF, D)
    parts = [(i // 2, ref, low if i % 2 else high) for i, ref in enumerate(refs)]
    return [
        (s, pltpu.make_async_copy(ref.at[:, lanes], target(s, rows), sems.at[i]))
        for i, (s, ref, rows) in enumerate(parts)
    ]


def hidden_kernel(rows, *args):
    refs, (out, x, w, sems) = args[: 2 * G], args[2 * G :]
    sets = [
        piece_copies(
            refs,
            slice(at, at + 2 * TILE),
            lambda s, r, j=j: w.at[j, s, r],
            sems.at[j],
        )
        for j, at in ((0, 0), (1, 3 * TILE))
    ]
    for copies in sets:
        for _, copy in copies:
            copy.start()
    for t in range(N_TP):
        x[:, t * TILE : (t + 1) * TILE] = rows[t]
    for j, part in ((0, slice(0, ROWS)), (1, slice(ROWS, ALL_ROWS))):
        full = x[part, :]
        scale = row_scale(full.astype(F32))
        for s in range(G):
            for step, copy in sets[j]:
                if step == s:
                    copy.wait()
            result = gated(scale, dot(full, w[j, s]))
            for k in range(G):
                out[k, part, s * TILE : (s + 1) * TILE] = result


def down_kernel(meta, hidden, *args):
    refs, (out, x, w, sems) = args[: 2 * G], args[2 * G :]
    sets = [
        piece_copies(
            refs,
            slice(at, at + TILE),
            lambda s, r, j=j: w.at[j, r, pl.ds(s * TILE, TILE)],
            sems.at[j],
        )
        for j, at in ((0, 2 * TILE), (1, 5 * TILE))
    ]
    for copies in sets:
        for _, copy in copies:
            copy.start()
    places = [lax.rem(meta[0] + (G - s), G) for s in range(G)]
    for s in range(G):
        for h in range(G):
            tile = places[s] * meta[2] + h * meta[3]
            x[:, lanes_at(tile)] = hidden[h, :, s * TILE : (s + 1) * TILE]
    for j, part in ((0, slice(0, ROWS)), (1, slice(ROWS, ALL_ROWS))):
        for _, copy in sets[j]:
            copy.wait()
        result = dot(x[part, :], w[j]).astype(BF)
        for s in range(G):
            out[places[s], part] = result[:, s * TILE : (s + 1) * TILE]


def return_kernel(parts, out):
    for r in range(G):
        out[r] = parts[r, :ROWS]


def combine_kernel(back, slots, weights_t, stream, parts, out):
    n = TOK_DEV
    own = jnp.concatenate([parts[r, ROWS:] for r in range(G)], axis=0)
    total = stream[...].astype(F32) + own.astype(F32)
    step = 256
    dims = (((0,), (0,)), ((), ()))
    for j in range(0, N_SP * CAP, step):
        place = lax.broadcasted_iota(jnp.int32, (step, n), 0) + j
        mix = jnp.where(place == slots[0:1, :], weights_t[0:1, :], 0.0) + jnp.where(
            place == slots[1:2, :], weights_t[1:2, :], 0.0
        )
        high = mix.astype(BF)
        low = (mix - high.astype(F32)).astype(BF)
        piece = back[j : j + step, :]
        total = total + dot(high, piece, dims) + dot(low, piece, dims)
    out[...] = total.astype(BF)


def layer(
    queries,
    keys_values,
    sink_logits,
    proj_weight,
    residual,
    norm_gain,
    routes,
    route_weights,
    gate_weight,
    up_weight,
    down_weight,
    shared_gate,
    shared_up,
    shared_down,
):
    sds = jax.ShapeDtypeStruct

    def kept(x):
        return pltpu.with_memory_space_constraint(x, pltpu.HBM)

    sp = lax.axis_index("sp")
    tp = lax.axis_index("tp")
    odd = lax.rem(sp, 2)
    high, low = tp // G, lax.rem(tp, G)
    r = jnp.where(odd == 0, high, low)
    h = jnp.where(odd == 0, low, high)
    meta = jnp.stack([r, h, jnp.where(odd == 0, G, 1), jnp.where(odd == 0, 1, G), sp]).astype(
        jnp.int32
    )

    payload = call(
        payload_kernel,
        sds((N_TP, WINDOW + HEAD_WIDTH + 16, TILE), BF),
        [SM, VM, HB],
        [pltpu.VMEM(proj_weight.shape, BF), pltpu.SemaphoreType.DMA],
    )(sink_logits, queries.T, kept(proj_weight))
    recv = lax.all_to_all(payload, "tp", 0, 0, tiled=True)
    halo = lax.ppermute(
        keys_values[:, TOK_DEV - WINDOW :, :], "sp", [(i, i + 1) for i in range(N_SP - 1)]
    )

    half = sds((HALF, 6 * TILE), BF)
    own_top, own_bottom = call(
        prep_kernel,
        (half, half),
        [VM] + [HB] * 6,
        [
            pltpu.VMEM((4, D, TILE), BF),
            pltpu.VMEM((4, D, TILE), BF),
            pltpu.SemaphoreType.DMA((16,)),
        ],
        outs=(HB, HB),
    )(
        norm_gain.reshape(N_TP, TILE),
        kept(gate_weight[0]),
        kept(up_weight[0]),
        kept(down_weight[0]),
        kept(shared_gate),
        kept(shared_up),
        kept(shared_down),
    )
    behind_top = shifted(own_top, R_GROUPS, 1)
    ahead_bottom = shifted(own_bottom, R_GROUPS, 3)
    behind_bottom = shifted(own_bottom, R_GROUPS, 1)
    ahead_top = shifted(own_top, R_GROUPS, 3)
    top = shifted(behind_top, R_GROUPS, 1)
    bottom = shifted(ahead_bottom, R_GROUPS, 3)
    weights = (
        own_top, own_bottom, behind_top, behind_bottom, top, bottom, ahead_top, ahead_bottom
    )

    rows = N_SP * CAP
    stream, picked, slots = call(
        front_kernel,
        (sds((TOK_DEV, TILE), BF), sds((rows, TILE), BF), sds((2, TOK_DEV), jnp.int32)),
        [SM, VM, HB, HB, HB, HB],
        [
            pltpu.VMEM(recv.shape, BF),
            pltpu.VMEM(halo.shape, BF),
            pltpu.VMEM(keys_values.shape, BF),
            pltpu.VMEM(residual.shape, BF),
            pltpu.VMEM((rows, TOK_DEV), BF),
            pltpu.VMEM((TOK_DEV, HEADS * HEAD_WIDTH), BF),
            pltpu.VMEM((rows, TILE), BF),
            pltpu.SemaphoreType.DMA((6,)),
        ],
        outs=(VM, HB, VM),
    )(meta, routes.T, kept(recv), kept(halo), kept(keys_values), kept(residual))

    arrived = lax.all_to_all(picked.reshape(N_SP, CAP, TILE), "sp", 0, 0, tiled=True)

    sent = call(spread_kernel, sds((N_TP, ALL_ROWS, TILE), BF), [SM, VM, VM])(
        meta, arrived.reshape(G, ROWS, TILE), stream.reshape(G, OWN, TILE)
    )
    rows = lax.all_to_all(sent, "tp", 0, 0, tiled=True)

    hidden = call(
        hidden_kernel,
        sds((G, ALL_ROWS, G * TILE), BF),
        [VM] + [HB] * (2 * G),
        [
            pltpu.VMEM((ALL_ROWS, D), BF),
            pltpu.VMEM((2, G, D, 2 * TILE), BF),
            pltpu.SemaphoreType.DMA((2, 2 * G)),
        ],
    )(rows, *weights)
    hidden = swapped(hidden, H_GROUPS)

    parts = call(
        down_kernel,
        sds((G, ALL_ROWS, TILE), BF),
        [SM, VM] + [HB] * (2 * G),
        [
            pltpu.VMEM((ALL_ROWS, D), BF),
            pltpu.VMEM((2, D, G * TILE), BF),
            pltpu.SemaphoreType.DMA((2, 2 * G)),
        ],
    )(meta, hidden, *weights)
    parts = swapped(parts, R_GROUPS)

    outgoing = call(return_kernel, sds((G, ROWS, TILE), BF), [VM])(parts)
    back = lax.all_to_all(outgoing.reshape(N_SP, CAP, TILE), "sp", 0, 0, tiled=True)
    return call(combine_kernel, sds((TOK_DEV, TILE), BF), [VM, VM, VM, VM, VM])(
        back.reshape(N_SP * CAP, TILE), slots, route_weights.T, stream, parts
    )


def solution(mesh):
    placed = (
        P("sp", "tp"),
        P(None, "sp", None),
        P("tp"),
        P("tp", None),
        P("sp", "tp"),
        P(),
        P("sp", None),
        P("sp", None),
        P("sp", None, "tp"),
        P("sp", None, "tp"),
        P("sp", None, "tp"),
        P(None, "tp"),
        P(None, "tp"),
        P(None, "tp"),
    )
    return jax.shard_map(
        layer, mesh=mesh, in_specs=placed, out_specs=P("sp", "tp"), check_vma=False
    )
```

time: 211 us -> 195 us (0.924)
  blocking collectives: 82.3 us -> 59.5 us
  starting transfers between devices: 41 us -> 53.9 us
  local copies, waits for them, and re-layouts: 14.5 us -> 4.09 us
  waiting for transfers between devices: 42.9 us -> 52.7 us
  other arithmetic: 6.95 us -> 0 us
    all_to_all x0 -> x1, waiting for transfers between devices: none -> 29.4 us  [layer(): rows = lax.all_to_all(sent, 'tp', 0, 0, tiled=True)]
    all_to_all x1 -> x0, blocking collectives: 23.6 us -> none  [layer(): rows = lax.all_to_all(sent, 'tp', 0, 0, tiled=True)]
    all_to_all x1, waiting for transfers between devices: 30.4 us -> 11.3 us  [layer(): recv = lax.all_to_all(payload, 'tp', 0, 0, tiled=True)]
    unnamed x4 -> x0, other arithmetic: 6.95 us -> none
    all_to_all x0 -> x1, starting transfers between devices: none -> 6.51 us  [layer(): rows = lax.all_to_all(sent, 'tp', 0, 0, tiled=True)]
    ppermute x4 -> x6, starting transfers between devices: 13.9 us -> 20.1 us  [shifted(): return lax.ppermute(x, BOTH, pairs)]
    unnamed x34 -> x18, local copies, waits for them, and re-layouts: 8.92 us -> 3.36 us
    slice x2 -> x0, local copies, waits for them, and re-layouts: 3.94 us -> none  [the longest x1 2.68 us: layer(): top = shifted(behind[:HALF], R_GROUPS, 1)]
  transfers between devices with their start and end apart: 7 -> 10, of which waited for: 3 -> 4; matrix products, arithmetic and copies ran while one was open for 2% -> 0% of each run, Pallas kernels for 5% -> 5%
where the time goes in v1:
time: 195 us; the launch traced here: 194 us
  blocking collectives  59.5 us (31%)
  starting transfers between devices  53.9 us (28%)
  waiting for transfers between devices  52.7 us (27%)
  Pallas kernels  23 us (12%)
  local copies, waits for them, and re-layouts  4.09 us (2%)
    all_to_all x1, blocking collectives, layer(): lax.all_to_all(outgoing.reshape(N_SP, CAP, TILE), 'sp', 0, 0, tiled=True)  37.6 us
    all_to_all x1, waiting for transfers between devices, layer(): rows = lax.all_to_all(sent, 'tp', 0, 0, tiled=True)  29.4 us
    all_to_all x2, blocking collectives, swapped(): return lax.all_to_all(x, BOTH, 0, 0, tiled=True, axis_index_groups=groups)  21.8 us
    ppermute x6, starting transfers between devices, shifted(): return lax.ppermute(x, BOTH, pairs)  20.1 us
    all_to_all x1, starting transfers between devices, layer(): lax.all_to_all(picked.reshape(N_SP, CAP, TILE), 'sp', 0, 0, tiled=True)  16.6 us
    all_to_all x1, waiting for transfers between devices, layer(): recv = lax.all_to_all(payload, 'tp', 0, 0, tiled=True)  11.3 us
    all_to_all x1, waiting for transfers between devices, layer(): lax.all_to_all(picked.reshape(N_SP, CAP, TILE), 'sp', 0, 0, tiled=True)  9.4 us
    pallas_call x1, Pallas kernels, layer(): call(front_kernel, (sds((TOK_DEV, TILE), BF), sds((rows, TILE), BF), sds(...  7.9 us
  transfers between devices with their start and end apart: 10, of which 4 were waited for; matrix products, arithmetic and copies ran while one was open for 0% of the time, Pallas kernels for 5%

profile of v1, /device:TPU:1, one launch (start us, length us, event | category | flops | bytes accessed | tf_op | source)
XLA Modules:
  0.0 194.1 jit_solution(10912981001225650540)
XLA Ops:
  0.0 0.0 copy-start.4
  0.0 0.7 copy-done.4
  0.7 2.2 %shard_map.139 = (bf16[1024,768]{1,0:T(8,128)(2,1)S(1)}, bf16[1024,768]{1,0:T(8,128)(2,1)S(1)}) custom-call(f32[16,128]{1,0:T(8,128)S(1)} %bitcast.23, bf16[2048,128]{1,0:T(8,128)(2,1)} %bitcast.26, bf16[2048,128]{1,0:T(8,128)(2,1)} %bitcast.27, bf16[2048,128]{1,0:T(8,128)(2,1)} %bitcast.28, bf16[2048,128]{1,0:T(8,128)(2,1)} %s_gate.1, ...), custom_call_target="tpu_custom_call" | custom-call | tf_op jit(solution)/shard_map/pallas_call | solution.py:371
  2.9 0.0 copy-start.7
  3.0 4.1 %collective-permute-start.1 = (bf16[1024,768]{1,0:T(8,128)(2,1)S(1)}, bf16[1024,768]{1,0:T(8,128)(2,1)}, u32[]{:S(2)}, u32[]{:S(2)}) collective-permute-start(bf16[1024,768]{1,0:T(8,128)(2,1)S(1)} %get-tuple-element.12.args_0_), channel_id=1, source_target_pairs={{0,4},{4,8},{8,12},{12,0},{1,5},{5,9},{9,13},{13,1},{2,6},{6,10},{... | collective-permute-start | bytes 4718600 | tf_op jit(solution)/shard_map/ppermute | solution.py:49
  7.0 3.2 %collective-permute-start.4 = (bf16[1024,768]{1,0:T(8,128)(2,1)S(1)}, bf16[1024,768]{1,0:T(8,128)(2,1)}, u32[]{:S(2)}, u32[]{:S(2)}) collective-permute-start(bf16[1024,768]{1,0:T(8,128)(2,1)S(1)} %get-tuple-element.13.args_1_), channel_id=1, source_target_pairs={{0,12},{4,0},{8,4},{12,8},{1,13},{5,1},{9,5},{13,9},{2,14},{6,2},{... | collective-permute-start | bytes 4718600 | tf_op jit(solution)/shard_map/ppermute | solution.py:49
  10.9 0.0 copy-done.3
  10.9 0.0 copy-start.5
  10.9 1.1 shard_map.136
  12.0 0.0 copy-start.1
  12.0 0.9 copy-done.1
  12.9 5.8 %all-to-all-start = ((bf16[16,208,128]{2,1,0:T(8,128)(2,1)}), bf16[16,208,128]{2,1,0:T(8,128)(2,1)}, u32[]{:S(2)}, u32[]{:S(2)}) async-start(bf16[16,208,128]{2,1,0:T(8,128)(2,1)} %copy-done.1), calls=%async_computation | async-start | bytes 1703936 | tf_op jit(solution)/shard_map/all_to_all | solution.py:365
  18.7 0.0 copy-done.7
  18.7 0.6 slice.3
  19.3 4.9 %collective-permute-start = (bf16[2,128,256]{2,1,0:T(8,128)(2,1)}, bf16[2,128,256]{2,1,0:T(8,128)(2,1)S(1)}, u32[]{:S(2)}, u32[]{:S(2)}) collective-permute-start(bf16[2,128,256]{2,1,0:T(8,128)(2,1)} %slice.3), channel_id=1, source_target_pairs={{0,16},{16,32},{32,48},{48,64},{64,80},{80,96},{96,112},{112,128},... | collective-permute-start | bytes 393224 | tf_op jit(solution)/shard_map/ppermute | solution.py:366
  24.3 0.1 stack.23.meta
  24.4 2.5 %collective-permute-done.halo_at = bf16[2,128,256]{2,1,0:T(8,128)(2,1)S(1)} collective-permute-done((bf16[2,128,256]{2,1,0:T(8,128)(2,1)}, bf16[2,128,256]{2,1,0:T(8,128)(2,1)S(1)}, u32[]{:S(2)}, u32[]{:S(2)}) %collective-permute-start) | collective-permute-done | bytes 131104 | tf_op jit(solution)/shard_map/ppermute | solution.py:366
  26.9 11.3 %all-to-all-done.recv_at = bf16[16,208,128]{2,1,0:T(8,128)(2,1)} async-done(((bf16[16,208,128]{2,1,0:T(8,128)(2,1)}), bf16[16,208,128]{2,1,0:T(8,128)(2,1)}, u32[]{:S(2)}, u32[]{:S(2)}) %all-to-all-start) | async-done | bytes 852000 | tf_op jit(solution)/shard_map/all_to_all | solution.py:365
  38.2 0.0 copy-done.8
  38.2 0.0 copy-done.5
  38.3 7.9 %shard_map.137 = (bf16[256,128]{1,0:T(8,128)(2,1)S(1)}, bf16[1024,128]{1,0:T(8,128)(2,1)S(1)}, s32[2,256]{1,0:T(2,128)S(1)}) custom-call(s32[5]{0:T(128)S(1)} %stack.23.meta, s32[2,256]{1,0:T(2,128)S(1)} %bitcast.24, bf16[16,208,128]{2,1,0:T(8,128)(2,1)} %all-to-all-done.recv_at, bf16[2,128,256]{2,1,0:T(8,128)(2,1)} %copy-done.8, ...), custom_call_target="tpu_custom_call" | custom-call | tf_op jit(solution)/shard_map/pallas_call | solution.py:401
  46.2 0.0 copy-start.2
  46.2 0.7 copy-done.2
  46.9 16.6 %all-to-all-start.1 = ((bf16[32,32,128]{2,1,0:T(8,128)(2,1)}), bf16[32,32,128]{2,1,0:T(8,128)(2,1)S(1)}, u32[]{:S(2)}, u32[]{:S(2)}) async-start(bf16[32,32,128]{2,1,0:T(8,128)(2,1)} %bitcast.20), calls=%async_computation.1 | async-start | bytes 524288 | tf_op jit(solution)/shard_map/all_to_all | solution.py:418
  63.5 4.4 %collective-permute-start.6 = (bf16[1024,768]{1,0:T(8,128)(2,1)S(1)}, bf16[1024,768]{1,0:T(8,128)(2,1)}, u32[]{:S(2)}, u32[]{:S(2)}) collective-permute-start(bf16[1024,768]{1,0:T(8,128)(2,1)S(1)} %get-tuple-element.12.args_0_), channel_id=1, source_target_pairs={{0,12},{4,0},{8,4},{12,8},{1,13},{5,1},{9,5},{13,9},{2,14},{6,2},{... | collective-permute-start | bytes 4718600 | tf_op jit(solution)/shard_map/ppermute | solution.py:49
  67.9 1.9 collective-permute-start.2
  69.8 0.0 collective-permute-done.1.args_2_
  69.8 3.2 %collective-permute-start.3 = (bf16[1024,768]{1,0:T(8,128)(2,1)}, bf16[1024,768]{1,0:T(8,128)(2,1)}, u32[]{:S(2)}, u32[]{:S(2)}) collective-permute-start(bf16[1024,768]{1,0:T(8,128)(2,1)} %collective-permute-done.1.args_2_), channel_id=1, source_target_pairs={{0,4},{4,8},{8,12},{12,0},{1,5},{5,9},{9,13},{13,1},{2,6},{6,10},{... | collective-permute-start | bytes 4718600 | tf_op jit(solution)/shard_map/ppermute | solution.py:49
  73.0 0.0 collective-permute-done.4.args_7_
  73.0 3.3 %collective-permute-start.5 = (bf16[1024,768]{1,0:T(8,128)(2,1)}, bf16[1024,768]{1,0:T(8,128)(2,1)}, u32[]{:S(2)}, u32[]{:S(2)}) collective-permute-start(bf16[1024,768]{1,0:T(8,128)(2,1)} %collective-permute-done.4.args_7_), channel_id=1, source_target_pairs={{0,12},{4,0},{8,4},{12,8},{1,13},{5,1},{9,5},{13,9},{2,14},{6,2},{... | collective-permute-start | bytes 4718600 | tf_op jit(solution)/shard_map/ppermute | solution.py:49
  76.3 9.4 %all-to-all-done.1 = bf16[32,32,128]{2,1,0:T(8,128)(2,1)S(1)} async-done(((bf16[32,32,128]{2,1,0:T(8,128)(2,1)}), bf16[32,32,128]{2,1,0:T(8,128)(2,1)S(1)}, u32[]{:S(2)}, u32[]{:S(2)}) %all-to-all-start.1) | async-done | bytes 262176 | tf_op jit(solution)/shard_map/all_to_all | solution.py:418
  85.7 0.6 shard_map.138
  86.4 0.0 copy-start
  86.4 1.0 copy-done
  87.4 6.5 %all-to-all-start.2 = ((bf16[16,320,128]{2,1,0:T(8,128)(2,1)}), bf16[16,320,128]{2,1,0:T(8,128)(2,1)}, u32[]{:S(2)}, u32[]{:S(2)}) async-start(bf16[16,320,128]{2,1,0:T(8,128)(2,1)} %copy-done), calls=%async_computation.2 | async-start | bytes 2621440 | tf_op jit(solution)/shard_map/all_to_all | solution.py:423
  93.9 0.0 collective-permute-done.6.args_6_
  93.9 0.0 collective-permute-done.2.args_3_
  94.0 29.4 %all-to-all-done.2.rows = bf16[16,320,128]{2,1,0:T(8,128)(2,1)} async-done(((bf16[16,320,128]{2,1,0:T(8,128)(2,1)}), bf16[16,320,128]{2,1,0:T(8,128)(2,1)}, u32[]{:S(2)}, u32[]{:S(2)}) %all-to-all-start.2) | async-done | bytes 1310752 | tf_op jit(solution)/shard_map/all_to_all | solution.py:423
  123.4 0.0 collective-permute-done.3.args_4_
  123.4 0.0 collective-permute-done.5.args_5_
  123.4 6.6 %shard_map.140 = bf16[4,320,512]{2,1,0:T(8,128)(2,1)S(1)} custom-call(bf16[16,320,128]{2,1,0:T(8,128)(2,1)} %all-to-all-done.2.rows, bf16[1024,768]{1,0:T(8,128)(2,1)S(1)} %get-tuple-element.12.args_0_, bf16[1024,768]{1,0:T(8,128)(2,1)S(1)} %get-tuple-element.13.args_1_, bf16[1024,768]{1,0:T(8,128)(2,1)} %collective-permute-done.1.args_2_, ...), custom_call_target="tpu_custom_call" | custom-call | tf_op jit(solution)/shard_map/pallas_call | solution.py:425
  130.0 13.6 %all_to_all.30.hidden = bf16[4,320,512]{2,1,0:T(8,128)(2,1)S(1)} all-to-all(bf16[4,320,512]{2,1,0:T(8,128)(2,1)S(1)} %shard_map.140), channel_id=1, replica_groups={{0,1,2,3},{4,5,6,7},{8,9,10,11},{12,13,14,15},{16,20,24,28},{17,21,25,2..., dimensions={0} | all-to-all | bytes 2621440 | tf_op jit(solution)/shard_map/all_to_all | solution.py:53
  143.6 3.4 %shard_map.141 = bf16[4,320,128]{2,1,0:T(8,128)(2,1)S(1)} custom-call(s32[5]{0:T(128)S(1)} %stack.23.meta, bf16[4,320,512]{2,1,0:T(8,128)(2,1)S(1)} %all_to_all.30.hidden, bf16[1024,768]{1,0:T(8,128)(2,1)S(1)} %get-tuple-element.12.args_0_, bf16[1024,768]{1,0:T(8,128)(2,1)S(1)} %get-tuple-element.13.args_1_, ...), custom_call_target="tpu_custom_call" | custom-call | tf_op jit(solution)/shard_map/pallas_call | solution.py:437
  147.0 0.0 copy-start.6
  147.0 8.3 %all_to_all.31.parts = bf16[4,320,128]{2,1,0:T(8,128)(2,1)S(1)} all-to-all(bf16[4,320,128]{2,1,0:T(8,128)(2,1)S(1)} %shard_map.141), channel_id=1, replica_groups={{0,4,8,12},{1,5,9,13},{2,6,10,14},{3,7,11,15},{16,17,18,19},{20,21,22,2..., dimensions={0} | all-to-all | bytes 655360 | tf_op jit(solution)/shard_map/all_to_all | solution.py:53
  155.3 37.6 %all_to_all.32 = bf16[32,32,128]{2,1,0:T(8,128)(2,1)S(1)} all-to-all(bf16[32,32,128]{2,1,0:T(8,128)(2,1)S(1)} %bitcast.17), channel_id=1, replica_groups=mesh['sp'=32,'tp'=16] {'sp'}, dimensions={0} | all-to-all | bytes 524288 | tf_op jit(solution)/shard_map/all_to_all | solution.py:450
  192.9 0.0 copy-done.6
  192.9 1.2 shard_map.143
  (3 shorter events, 0.0 us)
Async XLA Ops:
  0.0 0.7 copy-start.4
  0.7 10.2 %copy-start.3 = (bf16[256,64]{0,1:T(8,128)(2,1)S(1)}, bf16[256,64]{0,1:T(8,128)(2,1)}, u32[]{:S(2)}) copy-start(bf16[256,64]{0,1:T(8,128)(2,1)} %param.14) | copy-start | bytes 98308
  2.9 15.7 %copy-start.7 = (bf16[2,256,256]{2,1,0:T(8,128)(2,1)S(1)}, bf16[2,256,256]{2,1,0:T(8,128)(2,1)}, u32[]{:S(2)}) copy-start(bf16[2,256,256]{2,1,0:T(8,128)(2,1)} %kv_at.1) | copy-start | bytes 786436
  3.0 66.9 %collective-permute-start.1 = (bf16[1024,768]{1,0:T(8,128)(2,1)S(1)}, bf16[1024,768]{1,0:T(8,128)(2,1)}, u32[]{:S(2)}, u32[]{:S(2)}) collective-permute-start(bf16[1024,768]{1,0:T(8,128)(2,1)S(1)} %get-tuple-element.12.args_0_), channel_id=1, source_target_pairs={{0,4},{4,8},{8,12},{12,0},{1,5},{5,9},{9,13},{13,1},{2,6},{6,10},{... | collective-permute-start | bytes 4718600 | tf_op jit(solution)/shard_map/ppermute | solution.py:49
  7.0 66.0 %collective-permute-start.4 = (bf16[1024,768]{1,0:T(8,128)(2,1)S(1)}, bf16[1024,768]{1,0:T(8,128)(2,1)}, u32[]{:S(2)}, u32[]{:S(2)}) collective-permute-start(bf16[1024,768]{1,0:T(8,128)(2,1)S(1)} %get-tuple-element.13.args_1_), channel_id=1, source_target_pairs={{0,12},{4,0},{8,4},{12,8},{1,13},{5,1},{9,5},{13,9},{2,14},{6,2},{... | collective-permute-start | bytes 4718600 | tf_op jit(solution)/shard_map/ppermute | solution.py:49
  10.9 27.4 %copy-start.5 = (s32[256,2]{0,1:T(2,128)S(1)}, s32[256,2]{0,1:T(2,128)}, u32[]{:S(2)}) copy-start(s32[256,2]{0,1:T(2,128)} %param.20) | copy-start | bytes 6148
  12.0 0.9 copy-start.1
  12.9 25.4 %all-to-all-start = ((bf16[16,208,128]{2,1,0:T(8,128)(2,1)}), bf16[16,208,128]{2,1,0:T(8,128)(2,1)}, u32[]{:S(2)}, u32[]{:S(2)}) async-start(bf16[16,208,128]{2,1,0:T(8,128)(2,1)} %copy-done.1), calls=%async_computation | async-start | bytes 1703936 | tf_op jit(solution)/shard_map/all_to_all | solution.py:365
  19.3 7.6 %collective-permute-start = (bf16[2,128,256]{2,1,0:T(8,128)(2,1)}, bf16[2,128,256]{2,1,0:T(8,128)(2,1)S(1)}, u32[]{:S(2)}, u32[]{:S(2)}) collective-permute-start(bf16[2,128,256]{2,1,0:T(8,128)(2,1)} %slice.3), channel_id=1, source_target_pairs={{0,16},{16,32},{32,48},{48,64},{64,80},{80,96},{96,112},{112,128},... | collective-permute-start | bytes 393224 | tf_op jit(solution)/shard_map/ppermute | solution.py:366
  26.9 11.3 %copy-start.8 = (bf16[2,128,256]{2,1,0:T(8,128)(2,1)}, bf16[2,128,256]{2,1,0:T(8,128)(2,1)S(1)}, u32[]{:S(2)}) copy-start(bf16[2,128,256]{2,1,0:T(8,128)(2,1)S(1)} %collective-permute-done.halo_at) | copy-start | bytes 393220
  46.2 0.7 copy-start.2
  46.9 38.9 %all-to-all-start.1 = ((bf16[32,32,128]{2,1,0:T(8,128)(2,1)}), bf16[32,32,128]{2,1,0:T(8,128)(2,1)S(1)}, u32[]{:S(2)}, u32[]{:S(2)}) async-start(bf16[32,32,128]{2,1,0:T(8,128)(2,1)} %bitcast.20), calls=%async_computation.1 | async-start | bytes 524288 | tf_op jit(solution)/shard_map/all_to_all | solution.py:418
  63.5 30.4 %collective-permute-start.6 = (bf16[1024,768]{1,0:T(8,128)(2,1)S(1)}, bf16[1024,768]{1,0:T(8,128)(2,1)}, u32[]{:S(2)}, u32[]{:S(2)}) collective-permute-start(bf16[1024,768]{1,0:T(8,128)(2,1)S(1)} %get-tuple-element.12.args_0_), channel_id=1, source_target_pairs={{0,12},{4,0},{8,4},{12,8},{1,13},{5,1},{9,5},{13,9},{2,14},{6,2},{... | collective-permute-start | bytes 4718600 | tf_op jit(solution)/shard_map/ppermute | solution.py:49
  67.9 26.1 %collective-permute-start.2 = (bf16[1024,768]{1,0:T(8,128)(2,1)S(1)}, bf16[1024,768]{1,0:T(8,128)(2,1)}, u32[]{:S(2)}, u32[]{:S(2)}) collective-permute-start(bf16[1024,768]{1,0:T(8,128)(2,1)S(1)} %get-tuple-element.13.args_1_), channel_id=1, source_target_pairs={{0,4},{4,8},{8,12},{12,0},{1,5},{5,9},{9,13},{13,1},{2,6},{6,10},{... | collective-permute-start | bytes 4718600 | tf_op jit(solution)/shard_map/ppermute | solution.py:49
  69.8 53.6 %collective-permute-start.3 = (bf16[1024,768]{1,0:T(8,128)(2,1)}, bf16[1024,768]{1,0:T(8,128)(2,1)}, u32[]{:S(2)}, u32[]{:S(2)}) collective-permute-start(bf16[1024,768]{1,0:T(8,128)(2,1)} %collective-permute-done.1.args_2_), channel_id=1, source_target_pairs={{0,4},{4,8},{8,12},{12,0},{1,5},{5,9},{9,13},{13,1},{2,6},{6,10},{... | collective-permute-start | bytes 4718600 | tf_op jit(solution)/shard_map/ppermute | solution.py:49
  73.0 50.3 %collective-permute-start.5 = (bf16[1024,768]{1,0:T(8,128)(2,1)}, bf16[1024,768]{1,0:T(8,128)(2,1)}, u32[]{:S(2)}, u32[]{:S(2)}) collective-permute-start(bf16[1024,768]{1,0:T(8,128)(2,1)} %collective-permute-done.4.args_7_), channel_id=1, source_target_pairs={{0,12},{4,0},{8,4},{12,8},{1,13},{5,1},{9,5},{13,9},{2,14},{6,2},{... | collective-permute-start | bytes 4718600 | tf_op jit(solution)/shard_map/ppermute | solution.py:49
  86.4 1.0 copy-start
  87.4 36.0 %all-to-all-start.2 = ((bf16[16,320,128]{2,1,0:T(8,128)(2,1)}), bf16[16,320,128]{2,1,0:T(8,128)(2,1)}, u32[]{:S(2)}, u32[]{:S(2)}) async-start(bf16[16,320,128]{2,1,0:T(8,128)(2,1)} %copy-done), calls=%async_computation.2 | async-start | bytes 2621440 | tf_op jit(solution)/shard_map/all_to_all | solution.py:423
  147.0 45.9 %copy-start.6 = (f32[256,2]{0,1:T(2,128)S(1)}, f32[256,2]{0,1:T(2,128)}, u32[]{:S(2)}) copy-start(f32[256,2]{0,1:T(2,128)} %param.21) | copy-start | bytes 6148
